TPU v7x, 32 devices: a whole 2x2x4 slice. The times are simulated.
32 devices in a mesh: fs: 16 (over z, y, x), tp: 2 (over core).
Axes of the slice: x: 2, y: 2, z: 4, core: 2. Of those that a mesh axis runs over, the one named last changes fastest.
Arguments:
- cotangent: bfloat16 [2048, 2048], P('fs')
- values_first: bfloat16 [2048, 2048], P('fs', 'tp'), may hold values from -6 to 6
- values_second: bfloat16 [2048, 2048], P('fs', 'tp'), may hold values from -6 to 6
- head_lambda: float32 [16], P('tp'), may hold values from 0.3 to 0.8
- out_gain: float32 [128], replicated, may hold values from 0.3 to 3
- weight: float32 [2048, 2048], P('fs', 'tp'), may hold values from -0.125 to 0.125
- left_stat: float32 [2048, 2048], P('fs', 'tp'), as said below
- right_stat: float32 [16, 128, 128], P('tp')
- left_root: bfloat16 [2048, 2048], P('fs'), as said below
- right_root: bfloat16 [16, 128, 128], P('tp')
Outputs:
- update_step: float32 [2048, 2048], P('fs', 'tp')
- new_weight: float32 [2048, 2048], P('fs', 'tp')
- new_copy: bfloat16 [2048, 2048], P(None, 'tp')
- new_left_stat: float32 [2048, 2048], P('fs', 'tp')
- new_right_stat: float32 [16, 128, 128], P('tp')
Inputs may be any that keep to these rules, and one draw needn't show every extreme that they name: `left_root`: each of the 2048 x 2048 matrix and the 16 matrices of size 128 equals its transpose; the same holds for right_root. `left_stat`: the matrix and each of the 16 matrices equals its transpose; the same holds for right_stat.
All inputs are finite; a program needn't handle non-finite values.
Results may differ from a plain program's by a relative error of at most 0.007.
Values may be sent and summed in bfloat16 or wider, within the bound.
A program may use at most 64 MiB of HBM per device.

v0:
```python
import jax
import jax.numpy as jnp
from jax import lax
from jax.sharding import PartitionSpec as P

epsilon = 1e-06
decay_rate = 0.9
learn_rate = 0.01
output_scale = 0.2


def normalized(values_first, values_second, head_lambda, out_gain):
    token_count = values_first.shape[0]
    head_count = head_lambda.shape[0]
    head_size = out_gain.shape[0]
    first = values_first.astype(jnp.float32).reshape(token_count, head_count, head_size)
    second = values_second.astype(jnp.float32).reshape(token_count, head_count, head_size)
    difference = first - head_lambda[None, :, None] * second
    inverse = lax.rsqrt(jnp.mean(difference * difference, axis=-1, keepdims=True) + epsilon)
    scaled = difference * inverse * out_gain * output_scale
    return scaled.reshape(token_count, head_count * head_size).astype(jnp.bfloat16)


def by_head(matrix, head_count):
    return matrix.reshape(matrix.shape[0], head_count, matrix.shape[1] // head_count)


def head_products(matrix, head_count):
    heads = by_head(matrix, head_count)
    return jnp.einsum("rhi,rhj->hij", heads, heads, preferred_element_type=jnp.float32)


def shards(
    cotangent,
    values_first,
    values_second,
    head_lambda,
    out_gain,
    weight,
    left_stat,
    right_stat,
    left_root,
    right_root,
):
    head_count = head_lambda.shape[0]
    own_rows = weight.shape[0]
    own_cols = weight.shape[1]
    width = left_root.shape[1]
    total_cols = own_cols * lax.axis_size("tp")
    head_out = normalized(values_first, values_second, head_lambda, out_gain)
    contract_rows = (((0,), (0,)), ((), ()))
    contract_cols = (((1,), (1,)), ((), ()))
    gradient = lax.psum_scatter(
        lax.dot_general(cotangent, head_out, contract_rows, preferred_element_type=jnp.float32),
        "fs",
        scatter_dimension=0,
        tiled=True,
    )
    grad_half = gradient.astype(jnp.bfloat16)
    portion = lax.all_gather(grad_half, "fs", axis=0, tiled=True)
    left_acc = jnp.dot(left_root, portion, preferred_element_type=jnp.float32)
    products = lax.dot_general(
        grad_half, portion, contract_cols, preferred_element_type=jnp.float32
    )
    stat_cols = products
    right_acc = head_products(portion, head_count)
    left_acc, stat_cols, right_acc = (left_acc, stat_cols, right_acc)
    left_summed = lax.psum_scatter(
        stat_cols.astype(jnp.bfloat16), "tp", scatter_dimension=1, tiled=True
    ).astype(jnp.float32)
    new_left_stat = decay_rate * left_stat + (1.0 - decay_rate) / total_cols * left_summed
    new_right_stat = decay_rate * right_stat + (1.0 - decay_rate) / width * right_acc
    left_half = left_acc.astype(jnp.bfloat16)
    precond = jnp.einsum(
        "rhi,hij->rhj",
        by_head(left_half, head_count),
        right_root,
        preferred_element_type=jnp.float32,
    )
    precond = precond.reshape(own_rows, own_cols)
    grad_square, update_square = lax.psum(
        (jnp.sum(gradient * gradient), jnp.sum(precond * precond)), ("fs", "tp")
    )
    factor = jnp.sqrt((grad_square + epsilon) / (update_square + epsilon))
    update_step = factor * precond
    new_weight = weight - learn_rate * update_step
    new_copy = lax.all_gather(new_weight.astype(jnp.bfloat16), "fs", axis=0, tiled=True)
    return (update_step, new_weight, new_copy, new_left_stat, new_right_stat)


def solution(mesh):
    return jax.shard_map(
        shards,
        mesh=mesh,
        in_specs=(
            P("fs", None),
            P("fs", "tp"),
            P("fs", "tp"),
            P("tp"),
            P(),
            P("fs", "tp"),
            P("fs", "tp"),
            P("tp", None, None),
            P("fs", None),
            P("tp", None, None),
        ),
        out_specs=(P("fs", "tp"), P("fs", "tp"), P(None, "tp"), P("fs", "tp"), P("tp", None, None)),
        check_vma=False,
    )
```

profile of v0, /device:TPU:0, one launch (start us, length us, event | category | flops | bytes accessed | tf_op | source)
XLA Modules:
  0.0 429.0 jit_solution(1545737733516648169)
XLA Ops:
  7.2 0.0 copy-start
  7.2 0.0 copy-start.2
  7.2 0.0 copy-start.3
  7.2 0.0 reduce-scatter.3.cloned.1.call-start
  7.2 1.1 convert_bitcast_fusion.1
  8.3 0.1 copy.36
  8.4 1.0 convert_bitcast_fusion
  9.4 0.1 copy.37
  9.5 0.7 broadcast_bitcast_fusion
  10.3 0.8 fusion.5
  11.0 0.2 multiply_reduce_fusion.2
  11.3 0.1 copy.27
  11.4 0.2 mul.108
  11.6 0.0 copy-done
  11.7 0.0 copy-done.2
  11.7 0.0 copy-done.3
  11.7 4.6 %convolution_bitcast_fusion = f32[2048,1024]{0,1:T(8,128)} fusion(bf16[128,2048]{1,0:T(8,128)(2,1)S(1)} %copy-done, bf16[128,1024]{1,0:T(8,128)(2,1)S(1)} %copy-done.2, bf16[128,1024]{1,0:T(8,128)(2,1)S(1)} %copy-done.3, f32[16,8,8,128]{3,2,1,0:T(8,128)S(1)} %bitcast.37, f32[1024]{0:T(1024)S(1)} %get-tuple-element.28, f32[1024]{0:T(1024)S(1)} %get-tuple-element.29), kind=kOutput, calls=%fused_computation | convolution fusion | flops 537919488 | bytes 9969664 | tf_op jit(solution)/shard_map/dot_general | solution.py:54
  16.3 0.0 reduce-scatter.3.cloned.1.call-update
  16.3 0.0 copy-start.8
  16.3 0.0 all-gather.3.cloned.1.call-start
  16.4 180.7 %reduce-scatter.3.cloned.1.call-done = f32[128,1024]{0,1:T(8,128)} async-done(((f32[2048,1024]{0,1:T(8,128)}), f32[128,1024]{0,1:T(8,128)}) %reduce-scatter.3.cloned.1.call-update) | async-done | bytes 524304 | tf_op jit(solution)/shard_map/reduce_scatter | solution.py:53
  197.0 2.6 multiply_reduce_fusion.1
  199.6 0.0 all-gather.3.cloned.1.call-update
  199.6 0.0 reduce-scatter.5.cloned.1.call-start
  199.7 91.8 %all-gather.3.cloned.1.call-done = bf16[2048,1024]{0,1:T(8,128)(2,1)} async-done(((bf16[128,1024]{0,1:T(8,128)(2,1)}), bf16[2048,1024]{0,1:T(8,128)(2,1)}) %all-gather.3.cloned.1.call-update) | async-done | bytes 4194320 | tf_op jit(solution)/shard_map/all_gather | solution.py:60
  291.5 3.8 convolution_convert_fusion
  295.3 0.0 reduce-scatter.5.cloned.1.call-update
  295.3 0.0 copy-start.4
  295.3 0.0 all-gather.5.cloned.1.call-start
  295.4 0.0 copy-done.8
  295.4 3.5 convolution_convert_fusion.1
  298.9 0.0 copy-start.5
  298.9 0.0 copy-done.7
  298.9 0.9 multiply_reduce_fusion
  299.9 38.6 %all-reduce = (f32[]{:T(128)}, f32[]{:T(128)}) all-reduce(f32[]{:T(128)} %get-tuple-element.24, f32[]{:T(128)} %get-tuple-element.26), channel_id=1, replica_groups=mesh['fs'=16,'tp'=2] {'fs','tp'}, use_global_device_ids=true, to_apply=%region_3.0 | all-reduce | flops 2 | bytes 16 | tf_op jit(solution)/shard_map/psum | solution.py:81
  339.9 0.2 copy.32
  340.1 0.0 copy-done.4
  340.1 0.0 copy-start.1
  340.1 1.0 fusion.11
  341.2 0.0 all-gather.5.cloned.1.call-update
  341.2 0.0 copy-done.5
  341.2 0.0 copy-start.6
  341.2 5.6 %fusion = f32[8,128,128]{2,1,0:T(8,128)} fusion(bf16[2048,8,128]{0,2,1:T(8,128)(2,1)} %bitcast.36, f32[8,128,128]{2,1,0:T(8,128)S(1)} %copy-done.5), kind=kOutput, calls=%fused_computation.3 | convolution fusion | flops 537264128 | bytes 5242880 | tf_op jit(solution)/shard_map/rhi,rhj->hij/dot_general | solution.py:30
  346.8 0.0 copy-done.1
  346.8 0.0 copy-done.6
  346.8 1.8 multiply_add_fusion
  348.6 69.2 %all-gather.5.cloned.1.call-done = bf16[2048,1024]{1,0:T(8,128)(2,1)} async-done(((bf16[128,1024]{1,0:T(8,128)(2,1)}), bf16[2048,1024]{1,0:T(8,128)(2,1)}) %all-gather.5.cloned.1.call-update) | async-done | bytes 4194320 | tf_op jit(solution)/shard_map/all_gather | solution.py:87
  417.8 4.6 %copy.42 = bf16[2048,1024]{1,0:T(8,128)(2,1)} copy(bf16[2048,1024]{1,0:T(8,128)(2,1)} %all-gather.5.cloned.1.call-done) | data formatting | bytes 8388608
  (5 shorter events, 0.1 us)
Async XLA Ops:
  7.2 4.5 %copy-start = (bf16[128,2048]{1,0:T(8,128)(2,1)S(1)}, bf16[128,2048]{1,0:T(8,128)(2,1)}, u32[]{:S(2)}) copy-start(bf16[128,2048]{1,0:T(8,128)(2,1)} %param.10) | copy-start | bytes 1572868
  7.2 4.5 %copy-start.2 = (bf16[128,1024]{1,0:T(8,128)(2,1)S(1)}, bf16[128,1024]{1,0:T(8,128)(2,1)}, u32[]{:S(2)}) copy-start(bf16[128,1024]{1,0:T(8,128)(2,1)} %param.11) | copy-start | bytes 786436
  7.2 4.5 %copy-start.3 = (bf16[128,1024]{1,0:T(8,128)(2,1)S(1)}, bf16[128,1024]{1,0:T(8,128)(2,1)}, u32[]{:S(2)}) copy-start(bf16[128,1024]{1,0:T(8,128)(2,1)} %param.12) | copy-start | bytes 786436
  7.2 189.8 %reduce-scatter.3.cloned.1.call-start = ((), (), s32[]{:S(2)}) async-start(), calls=%async_computation.2 | async-start | bytes 8912896 | tf_op jit(solution)/shard_map/reduce_scatter | solution.py:53
  16.3 279.1 %copy-start.8 = (bf16[128,2048]{1,0:T(8,128)(2,1)S(1)}, bf16[128,2048]{1,0:T(8,128)(2,1)}, u32[]{:S(2)}) copy-start(bf16[128,2048]{1,0:T(8,128)(2,1)} %param.18) | copy-start | bytes 1572868
  16.3 275.2 %all-gather.3.cloned.1.call-start = ((), (), s32[]{:S(2)}) async-start(), calls=%async_computation.3 | async-start | bytes 4456448 | tf_op jit(solution)/shard_map/all_gather | solution.py:60
  199.6 147.2 %reduce-scatter.5.cloned.1.call-start = ((), (), s32[]{:S(2)}) async-start(), calls=%async_computation.5 | async-start | bytes 786432 | tf_op jit(solution)/shard_map/reduce_scatter | solution.py:68
  295.3 3.6 copy-start.7
  295.3 44.8 %copy-start.4 = (f32[128,1024]{1,0:T(8,128)S(1)}, f32[128,1024]{1,0:T(8,128)}, u32[]{:S(2)}) copy-start(f32[128,1024]{1,0:T(8,128)} %param.15) | copy-start | bytes 1572868
  295.3 122.5 %all-gather.5.cloned.1.call-start = ((), (), s32[]{:S(2)}) async-start(), calls=%async_computation.4 | async-start | bytes 4456448 | tf_op jit(solution)/shard_map/all_gather | solution.py:87
  298.9 42.3 %copy-start.5 = (f32[8,128,128]{2,1,0:T(8,128)S(1)}, f32[8,128,128]{2,1,0:T(8,128)}, u32[]{:S(2)}) copy-start(f32[8,128,128]{2,1,0:T(8,128)} %param.17) | copy-start | bytes 1572868
  340.1 6.7 %copy-start.1 = (f32[128,1024]{1,0:T(8,128)}, f32[128,1024]{1,0:T(8,128)S(1)}, u32[]{:S(2)}) copy-start(f32[128,1024]{1,0:T(8,128)S(1)} %copy.32) | copy-start | bytes 1572868
  341.2 5.6 %copy-start.6 = (f32[128,1024]{1,0:T(8,128)S(1)}, f32[128,1024]{1,0:T(8,128)}, u32[]{:S(2)}) copy-start(f32[128,1024]{1,0:T(8,128)} %param.16) | copy-start | bytes 1572868
Sparse Core Ops, SparseCore 0:
  16.4 180.5 reduce-scatter.2
  200.3 91.1 all-gather.2
  295.4 6.1 reduce-scatter.4
  341.3 76.4 all-gather.4
where the time goes:
time: 429 us
  waiting for transfers between devices  342 us (80%)
  blocking collectives  38.6 us (9%)
  matrix products  18.4 us (4%)
  between operations  15.3 us (4%)
  other arithmetic  8.5 us (2%)
  local copies, waits for them, and re-layouts  6.19 us (1%)
    reduce_scatter x1, waiting for transfers between devices, shards(): lax.psum_scatter(lax.dot_general(cotangent, head_out, contract_rows, pref...  181 us
    all_gather x1, waiting for transfers between devices, shards(): portion = lax.all_gather(grad_half, 'fs', axis=0, tiled=True)  91.8 us
    all_gather x1, waiting for transfers between devices, shards(): lax.all_gather(new_weight.astype(jnp.bfloat16), 'fs', axis=0, tiled=True)  69.2 us
    psum x1, blocking collectives, shards(): lax.psum((jnp.sum(gradient * gradient), jnp.sum(precond * precond)), ('fs...  38.6 us
  transfers between devices with their start and end apart: 4, of which 3 were waited for; matrix products, arithmetic and copies ran while one was open for 3% of the time, Pallas kernels for 0%

commit v1 on v0

--- a/solution.py
+++ b/solution.py
@@ -1,7 +1,14 @@
+import functools
+
 import jax
 import jax.numpy as jnp
 from jax import lax
+from jax.experimental import pallas as pl
+from jax.experimental.pallas import tpu as pltpu
 from jax.sharding import PartitionSpec as P
+
+MESH = pl.DeviceIdType.MESH
+INNER = 4
 
 epsilon = 1e-06
 decay_rate = 0.9
@@ -88,9 +95,398 @@
     return (update_step, new_weight, new_copy, new_left_stat, new_right_stat)
 
 
+def dot(a, b, dims):
+    return lax.dot_general(a, b, (dims, ((), ())), preferred_element_type=jnp.float32)
+
+
+def fused_kernel(
+    outer,
+    inner,
+    lam_ref,
+    cot_ref,
+    first_ref,
+    second_ref,
+    gain_ref,
+    root_ref,
+    right_root_hbm,
+    weight_hbm,
+    left_stat_hbm,
+    right_stat_hbm,
+    step_ref,
+    new_weight_ref,
+    copy_ref,
+    new_left_ref,
+    new_right_ref,
+    cot_all,
+    root_all,
+    head_out,
+    head_in,
+    part_out,
+    part_in,
+    grad_t,
+    grad_rows,
+    pre_out,
+    pre_in,
+    prod_all,
+    square_out,
+    square_in,
+    stat_own,
+    pair_out,
+    pair_in,
+    stat_out,
+    stat_in,
+    rr_ref,
+    w_ref,
+    ls_ref,
+    rs_ref,
+    send_sem,
+    recv_sem,
+    local_sem,
+):
+    me = lax.axis_index("fs")
+    core = lax.axis_index("tp")
+    oi = me // inner
+    ij = lax.rem(me, inner)
+    rows = cot_ref.shape[0]
+    width = cot_ref.shape[1]
+    own_rows = root_ref.shape[0]
+    size = gain_ref.shape[1]
+    cols = head_in.shape[1]
+    heads_each = cols // size
+    chunk = width // outer
+    half = width // 2
+    mine = pl.ds(pl.multiple_of(core * half, half), half)
+
+    def inner_peer(d):
+        return lax.rem(ij + d, inner)
+
+    def outer_peer(d):
+        return lax.rem(oi + d, outer)
+
+    def inner_id(d):
+        return (oi * inner + inner_peer(d), core)
+
+    def outer_id(d):
+        return (outer_peer(d) * inner + ij, core)
+
+    sibling = (me, 1 - core)
+    started = []
+
+    def send(src, dst, device):
+        index = len(started)
+        copy = pltpu.make_async_remote_copy(
+            src_ref=src,
+            dst_ref=dst,
+            send_sem=send_sem.at[index],
+            recv_sem=recv_sem.at[index],
+            device_id=device,
+            device_id_type=MESH,
+        )
+        copy.start()
+        started.append(copy)
+        return copy
+
+    inner_steps = range(1, inner)
+    outer_steps = range(1, outer)
+
+    locals_ = [
+        pltpu.make_async_copy(cot_ref, cot_all.at[ij], local_sem.at[0]),
+        pltpu.make_async_copy(root_ref, root_all.at[ij], local_sem.at[1]),
+        pltpu.make_async_copy(right_root_hbm, rr_ref, local_sem.at[2]),
+        pltpu.make_async_copy(weight_hbm, w_ref, local_sem.at[3]),
+        pltpu.make_async_copy(left_stat_hbm, ls_ref, local_sem.at[4]),
+        pltpu.make_async_copy(right_stat_hbm, rs_ref, local_sem.at[5]),
+    ]
+    for copy in locals_:
+        copy.start()
+
+    barrier = pltpu.get_barrier_semaphore()
+    peers = [inner_id(d) for d in inner_steps] + [outer_id(d) for d in outer_steps] + [sibling]
+    for peer in peers:
+        pl.semaphore_signal(barrier, inc=1, device_id=peer, device_id_type=MESH)
+    pl.semaphore_wait(barrier, len(peers))
+
+    cot_copies = [
+        send(cot_ref.at[:, mine], cot_all.at[ij, :, mine], inner_id(d)) for d in inner_steps
+    ]
+
+    gain = gain_ref[...] * output_scale
+    for h in range(inner * heads_each):
+        span = slice(h * size, (h + 1) * size)
+        first = first_ref[:, span].astype(jnp.float32)
+        second = second_ref[:, span].astype(jnp.float32)
+        difference = first - lam_ref[h] * second
+        inverse = lax.rsqrt(jnp.mean(difference * difference, axis=-1, keepdims=True) + epsilon)
+        scaled = difference * inverse * gain
+        k = h % heads_each
+        head_out[h // heads_each, k * size : (k + 1) * size, :] = scaled.T.astype(jnp.bfloat16)
+    head_copies = [
+        send(head_out.at[inner_peer(d)], head_in.at[ij], inner_id(d)) for d in inner_steps
+    ]
+    head_in[ij] = head_out[ij]
+
+    def forward(copies, buffer):
+        result = []
+        for d, copy in zip(inner_steps, copies):
+            copy.wait_recv()
+            place = buffer.at[lax.rem(ij + inner - d, inner), :, mine]
+            result.append(send(place, place, sibling))
+        return result
+
+    cot_pair = forward(cot_copies, cot_all)
+    for copy in head_copies:
+        copy.wait_recv()
+    root_copies = [
+        send(root_ref.at[:, mine], root_all.at[ij, :, mine], inner_id(d)) for d in inner_steps
+    ]
+    for copy in cot_pair:
+        copy.wait_recv()
+    locals_[0].wait()
+
+    lhs = jnp.concatenate([head_in[j] for j in range(inner)], axis=1)
+
+    def part(owner):
+        span = pl.ds(pl.multiple_of(owner * chunk, chunk), chunk)
+        rhs = cot_all[:, :, span].reshape(inner * rows, chunk)
+        return dot(lhs, rhs, ((1,), (0,)))
+
+    part_copies = []
+    for d in outer_steps:
+        owner = outer_peer(d)
+        part_out[d - 1] = part(owner).astype(jnp.bfloat16)
+        part_copies.append(send(part_out.at[d - 1], part_in.at[d - 1], outer_id(d)))
+    gradient = part(oi)
+    for d in outer_steps:
+        part_copies[d - 1].wait_recv()
+        gradient = gradient + part_in[d - 1].astype(jnp.float32)
+    grad_t[oi] = gradient.astype(jnp.bfloat16)
+    grad_copies = [send(grad_t.at[oi], grad_t.at[oi], outer_id(d)) for d in outer_steps]
+    square_out[0, 0] = jnp.full((8, 128), jnp.sum(gradient * gradient), jnp.float32)
+    grad_rows[...] = gradient.T.astype(jnp.bfloat16)
+
+    root_pair = forward(root_copies, root_all)
+    for copy in root_pair:
+        copy.wait_recv()
+    locals_[1].wait()
+    locals_[2].wait()
+    for copy in grad_copies:
+        copy.wait_recv()
+
+    total = jnp.zeros((1, 1), jnp.float32)
+    pre_copies = []
+    for d in tuple(inner_steps) + (0,):
+        block = inner_peer(d)
+        acc = jnp.zeros((own_rows, cols), jnp.float32)
+        for o in range(outer):
+            acc = acc + dot(
+                root_all[block, :, o * chunk : (o + 1) * chunk], grad_t[o], ((1,), (1,))
+            )
+        left_half = acc.astype(jnp.bfloat16)
+        for k in range(heads_each):
+            span = slice(k * size, (k + 1) * size)
+            precond = dot(left_half[:, span], rr_ref[ij * heads_each + k], ((1,), (0,)))
+            total = total + jnp.sum(precond * precond)
+            pre_out[block, :, span] = precond.astype(jnp.bfloat16)
+        if d:
+            pre_copies.append(send(pre_out.at[block], pre_in.at[ij], inner_id(d)))
+    pre_in[ij] = pre_out[ij]
+    square_out[0, 1] = jnp.broadcast_to(total, (8, 128))
+    square_copy = send(square_out.at[0], square_in.at[0], sibling)
+
+    def stat_part(core_half, k):
+        return dot(grad_rows[...], grad_t[core_half * (outer // 2) + k], ((1,), (0,)))
+
+    for k in range(outer // 2):
+        pair_out[:, k * chunk : (k + 1) * chunk] = stat_part(1 - core, k).astype(jnp.bfloat16)
+    pair_copy = send(pair_out, pair_in, sibling)
+
+    square_copy.wait_recv()
+    square_out[1] = square_out[0] + square_in[0]
+    square_copies = [
+        send(square_out.at[1], square_in.at[d], inner_id(d)) for d in inner_steps
+    ]
+    for k in range(heads_each):
+        product = jnp.zeros((size, size), jnp.float32)
+        for o in range(outer):
+            piece = grad_t[o, k * size : (k + 1) * size, :]
+            product = product + dot(piece, piece, ((1,), (1,)))
+        prod_all[ij, k] = product.astype(jnp.bfloat16)
+    prod_copies = [send(prod_all.at[ij], prod_all.at[ij], inner_id(d)) for d in inner_steps]
+
+    squares = square_out[1]
+    for d, copy in zip(inner_steps, square_copies):
+        copy.wait_recv()
+        squares = squares + square_in[d]
+    square_out[2] = squares
+    square_copies = [
+        send(square_out.at[2], square_in.at[inner + d - 1], outer_id(d)) for d in outer_steps
+    ]
+    for k in range(outer // 2):
+        stat_own[:, k * chunk : (k + 1) * chunk] = stat_part(core, k)
+
+    for copy in pre_copies:
+        copy.wait_recv()
+    locals_[3].wait()
+    for d, copy in zip(outer_steps, square_copies):
+        copy.wait_recv()
+        squares = squares + square_in[inner + d - 1]
+    factor = jnp.sqrt((squares[0] + epsilon) / (squares[1] + epsilon))[0:1, 0:1]
+
+    def rows_of(o, j):
+        return pl.ds(pl.multiple_of((o * inner + j) * own_rows, own_rows), own_rows)
+
+    place = rows_of(oi, ij)
+    for j in range(inner):
+        span = slice(j * cols, (j + 1) * cols)
+        step = factor * pre_in[j].astype(jnp.float32)
+        updated = w_ref[:, span] - learn_rate * step
+        step_ref[:, span] = step
+        new_weight_ref[:, span] = updated
+        copy_ref[place, span] = updated.astype(jnp.bfloat16)
+    own = copy_ref.at[place, :]
+    outer_copies = [send(own, own, outer_id(d)) for d in outer_steps]
+    inner_copies = [send(own, own, inner_id(d)) for d in inner_steps]
+
+    pair_copy.wait_recv()
+    stat_copies = []
+    for d in tuple(inner_steps) + (0,):
+        span = pl.ds(pl.multiple_of(inner_peer(d) * own_rows, own_rows), own_rows)
+        summed = stat_own[span, :] + pair_in[span, :].astype(jnp.float32)
+        if d:
+            stat_out[d - 1] = summed.astype(jnp.bfloat16)
+            stat_copies.append(send(stat_out.at[d - 1], stat_in.at[d - 1], inner_id(d)))
+        else:
+            stat_sum = summed
+
+    for d, copy in zip(outer_steps, outer_copies):
+        copy.wait_recv()
+        block = copy_ref.at[rows_of(lax.rem(oi + outer - d, outer), ij), :]
+        inner_copies += [send(block, block, inner_id(e)) for e in inner_steps]
+
+    for copy in prod_copies:
+        copy.wait_recv()
+    locals_[5].wait()
+    for j in range(inner):
+        for k in range(heads_each):
+            h = j * heads_each + k
+            new_right_ref[h] = decay_rate * rs_ref[h] + (1.0 - decay_rate) / width * prod_all[
+                j, k
+            ].astype(jnp.float32)
+    locals_[4].wait()
+    for copy in stat_copies:
+        copy.wait_recv()
+    for d in inner_steps:
+        stat_sum = stat_sum + stat_in[d - 1].astype(jnp.float32)
+    scale = (1.0 - decay_rate) / (2 * inner * cols)
+    new_left_ref[...] = decay_rate * ls_ref[...] + scale * stat_sum
+    for copy in inner_copies:
+        copy.wait_recv()
+    for copy in started:
+        copy.wait_send()
+
+
+def fused(
+    cotangent,
+    values_first,
+    values_second,
+    head_lambda,
+    out_gain,
+    weight,
+    left_stat,
+    right_stat,
+    left_root,
+    right_root,
+):
+    inner = INNER
+    outer = lax.axis_size("fs") // inner
+    rows, width = cotangent.shape
+    own_rows, own_cols = weight.shape
+    size = out_gain.shape[0]
+    cols = own_cols // inner
+    heads_each = cols // size
+    chunk = width // outer
+    half = width // 2
+    group_rows = inner * own_rows
+    bf16, f32 = jnp.bfloat16, jnp.float32
+    vmem = pl.BlockSpec(memory_space=pltpu.VMEM)
+    anywhere = pl.BlockSpec(memory_space=pl.ANY)
+    copies = 11 * (inner - 1) + 4 * (outer - 1) + (outer - 1) * (inner - 1) + 2
+    return pl.pallas_call(
+        functools.partial(fused_kernel, outer, inner),
+        out_shape=(
+            jax.ShapeDtypeStruct(weight.shape, f32),
+            jax.ShapeDtypeStruct(weight.shape, f32),
+            jax.ShapeDtypeStruct((width, own_cols), bf16),
+            jax.ShapeDtypeStruct(left_stat.shape, f32),
+            jax.ShapeDtypeStruct(right_stat.shape, f32),
+        ),
+        in_specs=[pl.BlockSpec(memory_space=pltpu.SMEM)] + [vmem] * 5 + [anywhere] * 4,
+        out_specs=[vmem] * 5,
+        scratch_shapes=[
+            pltpu.VMEM((inner, rows, width), bf16),
+            pltpu.VMEM((inner, own_rows, width), bf16),
+            pltpu.VMEM((inner, cols, rows), bf16),
+            pltpu.VMEM((inner, cols, rows), bf16),
+            pltpu.VMEM((outer - 1, cols, chunk), bf16),
+            pltpu.VMEM((outer - 1, cols, chunk), bf16),
+            pltpu.VMEM((outer, cols, chunk), bf16),
+            pltpu.VMEM((chunk, cols), bf16),
+            pltpu.VMEM((inner, own_rows, cols), bf16),
+            pltpu.VMEM((inner, own_rows, cols), bf16),
+            pltpu.VMEM((inner, heads_each, size, size), bf16),
+            pltpu.VMEM((3, 2, 8, 128), f32),
+            pltpu.VMEM((inner + outer - 1, 2, 8, 128), f32),
+            pltpu.VMEM((group_rows, half), f32),
+            pltpu.VMEM((group_rows, half), bf16),
+            pltpu.VMEM((group_rows, half), bf16),
+            pltpu.VMEM((inner - 1, own_rows, half), bf16),
+            pltpu.VMEM((inner - 1, own_rows, half), bf16),
+            pltpu.VMEM(right_root.shape, bf16),
+            pltpu.VMEM(weight.shape, f32),
+            pltpu.VMEM(left_stat.shape, f32),
+            pltpu.VMEM(right_stat.shape, f32),
+            pltpu.SemaphoreType.DMA((copies,)),
+            pltpu.SemaphoreType.DMA((copies,)),
+            pltpu.SemaphoreType.DMA((6,)),
+        ],
+        compiler_params=pltpu.CompilerParams(
+            collective_id=0, has_side_effects=True, vmem_limit_bytes=56 * 1024 * 1024
+        ),
+        name="fused_update",
+    )(
+        head_lambda,
+        cotangent,
+        values_first,
+        values_second,
+        out_gain.reshape(1, size),
+        left_root,
+        right_root,
+        weight,
+        left_stat,
+        right_stat,
+    )
+
+
+def step(*args):
+    head_count, size = args[3].shape[0], args[4].shape[0]
+    outer, rest = divmod(lax.axis_size("fs"), INNER)
+    aligned = (
+        rest == 0
+        and lax.axis_size("tp") == 2
+        and outer > 1
+        and outer % 2 == 0
+        and head_count % INNER == 0
+        and size == 128
+        and args[0].shape[0] % 128 == 0
+        and args[5].shape[0] % 16 == 0
+        and (args[0].shape[1] // outer) % 128 == 0
+    )
+    return tuple(fused(*args)) if aligned else shards(*args)
+
+
 def solution(mesh):
     return jax.shard_map(
-        shards,
+        step,
         mesh=mesh,
         in_specs=(
             P("fs", None),

time: 429 us -> 154 us (0.36)
  waiting for transfers between devices: 342 us -> 0 us
  Pallas kernels: 0 us -> 143 us
  blocking collectives: 38.6 us -> 0 us
  matrix products: 18.4 us -> 0 us
  between operations: 15.3 us -> 0.65 us
  other arithmetic: 8.5 us -> 0 us
    reduce_scatter x2 -> x0, waiting for transfers between devices: 181 us -> none  [the longest x1 181 us: shards(): lax.psum_scatter(lax.dot_general(cotangent, head_out, contract_rows, pref...]
    all_gather x2 -> x0, waiting for transfers between devices: 161 us -> none  [the longest x1 91.8 us: shards(): portion = lax.all_gather(grad_half, 'fs', axis=0, tiled=True)]
    pallas_call x0 -> x1, Pallas kernels: none -> 143 us  [fused(): pl.pallas_call(functools.partial(fused_kernel, outer, inner), out_shape=(...]
    psum x1 -> x0, blocking collectives: 38.6 us -> none  [shards(): lax.psum((jnp.sum(gradient * gradient), jnp.sum(precond * precond)), ('fs...]
    dot_general x5 -> x0, matrix products: 18.4 us -> none  [the longest x1 5.56 us: head_products(): jnp.einsum('rhi,rhj->hij', heads, heads, preferred_element_type=jnp.float32)]
    unnamed x22 -> x9, local copies, waits for them, and re-layouts: 5.08 us -> 10.1 us
  transfers between devices with their start and end apart: 4 -> 0, of which waited for: 3 -> 0; matrix products, arithmetic and copies ran while one was open for 3% -> 0% of each run, Pallas kernels for 0% -> 0%
where the time goes in v1:
time: 154 us
  Pallas kernels  143 us (93%)
  local copies, waits for them, and re-layouts  10.1 us (7%)
    pallas_call x1, Pallas kernels, fused(): pl.pallas_call(functools.partial(fused_kernel, outer, inner), out_shape=(...  143 us
    unnamed x9, local copies, waits for them, and re-layouts  10.1 us

profile of v1, /device:TPU:0, one launch (start us, length us, event | category | flops | bytes accessed | tf_op | source)
XLA Modules:
  0.0 153.9 jit_solution(9193432019421161717)
XLA Ops:
  0.6 143.2 %fused_update.1 = (f32[128,1024]{1,0:T(8,128)}, f32[128,1024]{1,0:T(8,128)}, bf16[2048,1024]{1,0:T(8,128)(2,1)}, f32[128,1024]{1,0:T(8,128)}, f32[8,128,128]{2,1,0:T(8,128)}) custom-call(f32[8]{0:T(128)} %lam_ref.1, bf16[128,2048]{1,0:T(8,128)(2,1)} %cot_ref.1, bf16[128,1024]{1,0:T(8,128)(2,1)} %first_ref.1, bf16[128,1024]{1,0:T(8,128)(2,1)} %second_ref.1, ...), custom_call_target="tpu_custom_call" | custom-call | tf_op jit(solution)/shard_map/fused_update/pallas_call | solution.py:414
  143.8 1.9 %copy.20 = f32[128,1024]{1,0:T(8,128)} copy(f32[128,1024]{1,0:T(8,128)} %get-tuple-element.10) | data formatting | bytes 1048576
  145.7 1.9 %copy.21 = f32[128,1024]{1,0:T(8,128)} copy(f32[128,1024]{1,0:T(8,128)} %get-tuple-element.11) | data formatting | bytes 1048576
  147.6 0.0 copy-start.1
  147.6 0.0 copy-start
  147.6 4.7 %copy.22 = bf16[2048,1024]{1,0:T(8,128)(2,1)} copy(bf16[2048,1024]{1,0:T(8,128)(2,1)} %get-tuple-element.12) | data formatting | bytes 8388608
  152.3 0.0 copy-done.1
  152.3 0.8 copy.23
  153.1 0.0 copy-done
  153.1 0.8 copy.24
Async XLA Ops:
  147.6 4.7 %copy-start.1 = (f32[128,1024]{1,0:T(8,128)S(1)}, f32[128,1024]{1,0:T(8,128)}, u32[]{:S(2)}) copy-start(f32[128,1024]{1,0:T(8,128)} %get-tuple-element.13) | copy-start | bytes 1572868
  147.6 5.5 %copy-start = (f32[8,128,128]{2,1,0:T(8,128)S(1)}, f32[8,128,128]{2,1,0:T(8,128)}, u32[]{:S(2)}) copy-start(f32[8,128,128]{2,1,0:T(8,128)} %get-tuple-element.14) | copy-start | bytes 1572868

commit v2 on v1

--- a/solution.py
+++ b/solution.py
@@ -103,11 +103,11 @@
     outer,
     inner,
     lam_ref,
-    cot_ref,
-    first_ref,
-    second_ref,
     gain_ref,
-    root_ref,
+    cot_hbm,
+    first_hbm,
+    second_hbm,
+    root_hbm,
     right_root_hbm,
     weight_hbm,
     left_stat_hbm,
@@ -123,6 +123,7 @@
     head_in,
     part_out,
     part_in,
+    own_part,
     grad_t,
     grad_rows,
     pre_out,
@@ -135,6 +136,8 @@
     pair_in,
     stat_out,
     stat_in,
+    first_ref,
+    second_ref,
     rr_ref,
     w_ref,
     ls_ref,
@@ -147,9 +150,8 @@
     core = lax.axis_index("tp")
     oi = me // inner
     ij = lax.rem(me, inner)
-    rows = cot_ref.shape[0]
-    width = cot_ref.shape[1]
-    own_rows = root_ref.shape[0]
+    rows, width = cot_hbm.shape
+    own_rows = root_hbm.shape[0]
     size = gain_ref.shape[1]
     cols = head_in.shape[1]
     heads_each = cols // size
@@ -160,55 +162,112 @@
     def inner_peer(d):
         return lax.rem(ij + d, inner)
 
-    def outer_peer(d):
-        return lax.rem(oi + d, outer)
+    is_mid = lax.rem((oi + 1) // 2, 2)
+    near = oi + 1 - 2 * lax.rem(oi, 2)
+    across = 2 - oi // 2
+    far = (outer - 1) * (1 - oi // 2)
+    x_peer = ij + 1 - 2 * lax.rem(ij, 2)
+    y_peer = lax.rem(ij + 2, inner)
 
     def inner_id(d):
         return (oi * inner + inner_peer(d), core)
 
-    def outer_id(d):
-        return (outer_peer(d) * inner + ij, core)
+    def outer_id(o):
+        return (o * inner + ij, core)
+
+    def inner_at(j):
+        return (oi * inner + j, core)
 
     sibling = (me, 1 - core)
     started = []
-
-    def send(src, dst, device):
-        index = len(started)
-        copy = pltpu.make_async_remote_copy(
+    started_mid = []
+    used = [0]
+
+    def fresh(count=1):
+        used[0] += count
+        return used[0] - count
+
+    def describe(src, dst, device, arrival):
+        return pltpu.make_async_remote_copy(
             src_ref=src,
             dst_ref=dst,
-            send_sem=send_sem.at[index],
-            recv_sem=recv_sem.at[index],
+            send_sem=send_sem.at[fresh()],
+            recv_sem=recv_sem.at[arrival],
             device_id=device,
             device_id_type=MESH,
         )
+
+    arrivals = [0]
+
+    def expect(count=1):
+        arrivals[0] += count
+        return arrivals[0] - count
+
+    def send(src, dst, device, arrival=None):
+        copy = describe(src, dst, device, expect() if arrival is None else arrival)
         copy.start()
         started.append(copy)
         return copy
 
+    def arrived(ref, arrival):
+        pltpu.make_async_copy(ref, ref, recv_sem.at[arrival]).wait()
+
+    def gather_outer(block):
+        base = expect(3)
+        own = block(oi)
+        send(own, own, outer_id(across), base + 1 + is_mid)
+        direct = describe(own, own, outer_id(far), base + 2)
+        relayed = describe(block(far), block(far), outer_id(near), base + 1)
+
+        @pl.when(is_mid == 1)
+        def _():
+            direct.start()
+
+        send(own, own, outer_id(near), base)
+        started_mid.extend([direct, relayed])
+
+        def wait_near():
+            arrived(block(near), base)
+
+        def wait_far():
+            arrived(block(far), base + 1)
+
+            @pl.when(is_mid == 1)
+            def _():
+                relayed.start()
+
+        def wait_across():
+            arrived(block(across), base + 2)
+
+        return wait_near, wait_far, wait_across
+
     inner_steps = range(1, inner)
     outer_steps = range(1, outer)
 
     locals_ = [
-        pltpu.make_async_copy(cot_ref, cot_all.at[ij], local_sem.at[0]),
-        pltpu.make_async_copy(root_ref, root_all.at[ij], local_sem.at[1]),
+        pltpu.make_async_copy(cot_hbm, cot_all.at[ij], local_sem.at[0]),
+        pltpu.make_async_copy(root_hbm, root_all.at[ij], local_sem.at[1]),
         pltpu.make_async_copy(right_root_hbm, rr_ref, local_sem.at[2]),
         pltpu.make_async_copy(weight_hbm, w_ref, local_sem.at[3]),
         pltpu.make_async_copy(left_stat_hbm, ls_ref, local_sem.at[4]),
         pltpu.make_async_copy(right_stat_hbm, rs_ref, local_sem.at[5]),
+        pltpu.make_async_copy(first_hbm, first_ref, local_sem.at[6]),
+        pltpu.make_async_copy(second_hbm, second_ref, local_sem.at[7]),
     ]
-    for copy in locals_:
-        copy.start()
+    for index in (0, 6, 7, 1, 2, 3, 4, 5):
+        locals_[index].start()
 
     barrier = pltpu.get_barrier_semaphore()
-    peers = [inner_id(d) for d in inner_steps] + [outer_id(d) for d in outer_steps] + [sibling]
+    peers = [inner_id(d) for d in inner_steps] + [outer_id(lax.rem(oi + d, outer)) for d in outer_steps] + [sibling]
     for peer in peers:
         pl.semaphore_signal(barrier, inc=1, device_id=peer, device_id_type=MESH)
     pl.semaphore_wait(barrier, len(peers))
 
-    cot_copies = [
-        send(cot_ref.at[:, mine], cot_all.at[ij, :, mine], inner_id(d)) for d in inner_steps
-    ]
+    locals_[0].wait()
+    own_cot = cot_all.at[ij, :, mine]
+    cot_copies = [send(own_cot, own_cot, inner_id(d)) for d in inner_steps]
+    locals_[6].wait()
+    locals_[7].wait()
 
     gain = gain_ref[...] * output_scale
     for h in range(inner * heads_each):
@@ -236,12 +295,11 @@
     cot_pair = forward(cot_copies, cot_all)
     for copy in head_copies:
         copy.wait_recv()
-    root_copies = [
-        send(root_ref.at[:, mine], root_all.at[ij, :, mine], inner_id(d)) for d in inner_steps
-    ]
+    locals_[1].wait()
+    own_root = root_all.at[ij, :, mine]
+    root_copies = [send(own_root, own_root, inner_id(d)) for d in inner_steps]
     for copy in cot_pair:
         copy.wait_recv()
-    locals_[0].wait()
 
     lhs = jnp.concatenate([head_in[j] for j in range(inner)], axis=1)
 
@@ -250,27 +308,51 @@
         rhs = cot_all[:, :, span].reshape(inner * rows, chunk)
         return dot(lhs, rhs, ((1,), (0,)))
 
-    part_copies = []
-    for d in outer_steps:
-        owner = outer_peer(d)
-        part_out[d - 1] = part(owner).astype(jnp.bfloat16)
-        part_copies.append(send(part_out.at[d - 1], part_in.at[d - 1], outer_id(d)))
-    gradient = part(oi)
-    for d in outer_steps:
-        part_copies[d - 1].wait_recv()
-        gradient = gradient + part_in[d - 1].astype(jnp.float32)
+    base = expect(4)
+    part_out[0] = part(far).astype(jnp.bfloat16)
+    to_relay = describe(part_out.at[0], part_in.at[3], outer_id(near), base + 3)
+
+    @pl.when(is_mid == 0)
+    def _():
+        to_relay.start()
+
+    part_out[1] = part(across).astype(jnp.bfloat16)
+    slot = 2 - is_mid
+    send(part_out.at[1], part_in.at[slot], outer_id(across), base + slot)
+    part_out[2] = part(near).astype(jnp.bfloat16)
+    send(part_out.at[2], part_in.at[0], outer_id(near), base)
+    combined = describe(part_out.at[3], part_in.at[1], outer_id(far), base + 1)
+
+    @pl.when(is_mid == 1)
+    def _():
+        arrived(part_in.at[3], base + 3)
+        total_far = part(far) + part_in[3].astype(jnp.float32)
+        part_out[3] = total_far.astype(jnp.bfloat16)
+        combined.start()
+
+    own_part[...] = part(oi)
+    arrived(part_in.at[0], base)
+    own_part[...] += part_in[0].astype(jnp.float32)
+
+    @pl.when(is_mid == 1)
+    def _():
+        arrived(part_in.at[2], base + 2)
+        own_part[...] += part_in[2].astype(jnp.float32)
+
+    arrived(part_in.at[1], base + 1)
+    gradient = own_part[...] + part_in[1].astype(jnp.float32)
     grad_t[oi] = gradient.astype(jnp.bfloat16)
-    grad_copies = [send(grad_t.at[oi], grad_t.at[oi], outer_id(d)) for d in outer_steps]
+    wait_near, wait_far, wait_across = gather_outer(lambda o: grad_t.at[o])
     square_out[0, 0] = jnp.full((8, 128), jnp.sum(gradient * gradient), jnp.float32)
     grad_rows[...] = gradient.T.astype(jnp.bfloat16)
 
     root_pair = forward(root_copies, root_all)
+    wait_far()
     for copy in root_pair:
         copy.wait_recv()
-    locals_[1].wait()
     locals_[2].wait()
-    for copy in grad_copies:
-        copy.wait_recv()
+    wait_near()
+    wait_across()
 
     total = jnp.zeros((1, 1), jnp.float32)
     pre_copies = []
@@ -319,33 +401,15 @@
         squares = squares + square_in[d]
     square_out[2] = squares
     square_copies = [
-        send(square_out.at[2], square_in.at[inner + d - 1], outer_id(d)) for d in outer_steps
+        send(
+            square_out.at[2],
+            square_in.at[inner + d - 1],
+            outer_id(lax.rem(oi + d, outer)),
+        )
+        for d in outer_steps
     ]
     for k in range(outer // 2):
         stat_own[:, k * chunk : (k + 1) * chunk] = stat_part(core, k)
-
-    for copy in pre_copies:
-        copy.wait_recv()
-    locals_[3].wait()
-    for d, copy in zip(outer_steps, square_copies):
-        copy.wait_recv()
-        squares = squares + square_in[inner + d - 1]
-    factor = jnp.sqrt((squares[0] + epsilon) / (squares[1] + epsilon))[0:1, 0:1]
-
-    def rows_of(o, j):
-        return pl.ds(pl.multiple_of((o * inner + j) * own_rows, own_rows), own_rows)
-
-    place = rows_of(oi, ij)
-    for j in range(inner):
-        span = slice(j * cols, (j + 1) * cols)
-        step = factor * pre_in[j].astype(jnp.float32)
-        updated = w_ref[:, span] - learn_rate * step
-        step_ref[:, span] = step
-        new_weight_ref[:, span] = updated
-        copy_ref[place, span] = updated.astype(jnp.bfloat16)
-    own = copy_ref.at[place, :]
-    outer_copies = [send(own, own, outer_id(d)) for d in outer_steps]
-    inner_copies = [send(own, own, inner_id(d)) for d in inner_steps]
 
     pair_copy.wait_recv()
     stat_copies = []
@@ -356,12 +420,64 @@
             stat_out[d - 1] = summed.astype(jnp.bfloat16)
             stat_copies.append(send(stat_out.at[d - 1], stat_in.at[d - 1], inner_id(d)))
         else:
-            stat_sum = summed
-
-    for d, copy in zip(outer_steps, outer_copies):
-        copy.wait_recv()
-        block = copy_ref.at[rows_of(lax.rem(oi + outer - d, outer), ij), :]
-        inner_copies += [send(block, block, inner_id(e)) for e in inner_steps]
+            stat_own[span, :] = summed
+
+    for copy in pre_copies:
+        copy.wait_recv()
+    locals_[3].wait()
+    for d, copy in zip(outer_steps, square_copies):
+        copy.wait_recv()
+        squares = squares + square_in[inner + d - 1]
+    factor = jnp.sqrt((squares[0] + epsilon) / (squares[1] + epsilon))[0:1, 0:1]
+
+    def rows_of(o, j):
+        return pl.ds(pl.multiple_of((o * inner + j) * own_rows, own_rows), own_rows)
+
+    place = rows_of(oi, ij)
+    for j in range(inner):
+        span = slice(j * cols, (j + 1) * cols)
+        step = factor * pre_in[j].astype(jnp.float32)
+        updated = w_ref[:, span] - learn_rate * step
+        step_ref[:, span] = step
+        new_weight_ref[:, span] = updated
+        copy_ref[place, span] = updated.astype(jnp.bfloat16)
+    near_in, far_in, across_in = gather_outer(lambda o: copy_ref.at[rows_of(o, ij), :])
+
+    def halves(o, j):
+        start = (o * inner + j) * own_rows
+        return [
+            copy_ref.at[pl.ds(pl.multiple_of(start + k * (own_rows // 2), own_rows // 2), own_rows // 2), :]
+            for k in range(2)
+        ]
+
+    flight = []
+
+    def spread(o):
+        block = copy_ref.at[rows_of(o, ij), :]
+        flight.append((o, send(block, block, inner_at(x_peer)), send(block, block, inner_at(y_peer))))
+
+    last = []
+
+    def pass_on(index):
+        o, from_x, from_y = flight[index]
+        from_x.wait_recv()
+        piece = halves(o, x_peer)[0]
+        last.append(send(piece, piece, inner_at(y_peer)))
+        from_y.wait_recv()
+        piece = halves(o, y_peer)[1]
+        last.append(send(piece, piece, inner_at(x_peer)))
+
+    spread(oi)
+    near_in()
+    spread(near)
+    pass_on(0)
+    far_in()
+    across_in()
+    spread(across)
+    pass_on(1)
+    spread(far)
+    pass_on(2)
+    pass_on(3)
 
     for copy in prod_copies:
         copy.wait_recv()
@@ -375,14 +491,25 @@
     locals_[4].wait()
     for copy in stat_copies:
         copy.wait_recv()
+    stat_sum = stat_own[pl.ds(pl.multiple_of(ij * own_rows, own_rows), own_rows), :]
     for d in inner_steps:
         stat_sum = stat_sum + stat_in[d - 1].astype(jnp.float32)
     scale = (1.0 - decay_rate) / (2 * inner * cols)
     new_left_ref[...] = decay_rate * ls_ref[...] + scale * stat_sum
-    for copy in inner_copies:
+    for copy in last:
         copy.wait_recv()
     for copy in started:
         copy.wait_send()
+
+    @pl.when(is_mid == 1)
+    def _():
+        combined.wait_send()
+        for copy in started_mid:
+            copy.wait_send()
+
+    @pl.when(is_mid == 0)
+    def _():
+        to_relay.wait_send()
 
 
 def fused(
@@ -410,25 +537,26 @@
     bf16, f32 = jnp.bfloat16, jnp.float32
     vmem = pl.BlockSpec(memory_space=pltpu.VMEM)
     anywhere = pl.BlockSpec(memory_space=pl.ANY)
-    copies = 11 * (inner - 1) + 4 * (outer - 1) + (outer - 1) * (inner - 1) + 2
+    copies = 12 * inner + 5 * outer + 4 * outer
     return pl.pallas_call(
         functools.partial(fused_kernel, outer, inner),
         out_shape=(
-            jax.ShapeDtypeStruct(weight.shape, f32),
-            jax.ShapeDtypeStruct(weight.shape, f32),
-            jax.ShapeDtypeStruct((width, own_cols), bf16),
-            jax.ShapeDtypeStruct(left_stat.shape, f32),
-            jax.ShapeDtypeStruct(right_stat.shape, f32),
+            pltpu.VMEM(weight.shape, f32),
+            pltpu.VMEM(weight.shape, f32),
+            pltpu.VMEM((width, own_cols), bf16),
+            pltpu.VMEM(left_stat.shape, f32),
+            pltpu.VMEM(right_stat.shape, f32),
         ),
-        in_specs=[pl.BlockSpec(memory_space=pltpu.SMEM)] + [vmem] * 5 + [anywhere] * 4,
+        in_specs=[pl.BlockSpec(memory_space=pltpu.SMEM)] + [vmem] + [anywhere] * 8,
         out_specs=[vmem] * 5,
         scratch_shapes=[
             pltpu.VMEM((inner, rows, width), bf16),
             pltpu.VMEM((inner, own_rows, width), bf16),
             pltpu.VMEM((inner, cols, rows), bf16),
             pltpu.VMEM((inner, cols, rows), bf16),
-            pltpu.VMEM((outer - 1, cols, chunk), bf16),
-            pltpu.VMEM((outer - 1, cols, chunk), bf16),
+            pltpu.VMEM((outer, cols, chunk), bf16),
+            pltpu.VMEM((outer, cols, chunk), bf16),
+            pltpu.VMEM((cols, chunk), f32),
             pltpu.VMEM((outer, cols, chunk), bf16),
             pltpu.VMEM((chunk, cols), bf16),
             pltpu.VMEM((inner, own_rows, cols), bf16),
@@ -441,13 +569,15 @@
             pltpu.VMEM((group_rows, half), bf16),
             pltpu.VMEM((inner - 1, own_rows, half), bf16),
             pltpu.VMEM((inner - 1, own_rows, half), bf16),
+            pltpu.VMEM(values_first.shape, bf16),
+            pltpu.VMEM(values_second.shape, bf16),
             pltpu.VMEM(right_root.shape, bf16),
             pltpu.VMEM(weight.shape, f32),
             pltpu.VMEM(left_stat.shape, f32),
             pltpu.VMEM(right_stat.shape, f32),
             pltpu.SemaphoreType.DMA((copies,)),
             pltpu.SemaphoreType.DMA((copies,)),
-            pltpu.SemaphoreType.DMA((6,)),
+            pltpu.SemaphoreType.DMA((8,)),
         ],
         compiler_params=pltpu.CompilerParams(
             collective_id=0, has_side_effects=True, vmem_limit_bytes=56 * 1024 * 1024
@@ -455,10 +585,10 @@
         name="fused_update",
     )(
         head_lambda,
+        out_gain.reshape(1, size),
         cotangent,
         values_first,
         values_second,
-        out_gain.reshape(1, size),
         left_root,
         right_root,
         weight,
@@ -473,8 +603,7 @@
     aligned = (
         rest == 0
         and lax.axis_size("tp") == 2
-        and outer > 1
-        and outer % 2 == 0
+        and outer == 4
         and head_count % INNER == 0
         and size == 128
         and args[0].shape[0] % 128 == 0

time: 154 us -> 126 us (0.82)
  Pallas kernels: 143 us -> 120 us
  local copies, waits for them, and re-layouts: 10.1 us -> 5.19 us
    pallas_call x1, Pallas kernels: 143 us -> 120 us  [fused(): pl.pallas_call(functools.partial(fused_kernel, outer, inner), out_shape=(...]
    unnamed x9 -> x5, local copies, waits for them, and re-layouts: 10.1 us -> 5.19 us
where the time goes in v2:
time: 126 us
  Pallas kernels  120 us (95%)
  local copies, waits for them, and re-layouts  5.19 us (4%)
    pallas_call x1, Pallas kernels, fused(): pl.pallas_call(functools.partial(fused_kernel, outer, inner), out_shape=(...  120 us
    unnamed x5, local copies, waits for them, and re-layouts  5.19 us

profile of v2, /device:TPU:0, one launch (start us, length us, event | category | flops | bytes accessed | tf_op | source)
XLA Modules:
  0.0 125.7 jit_solution(14670258375118083112)
XLA Ops:
  0.6 119.9 %fused_update.1 = (f32[128,1024]{1,0:T(8,128)S(1)}, f32[128,1024]{1,0:T(8,128)S(1)}, bf16[2048,1024]{1,0:T(8,128)(2,1)S(1)}, f32[128,1024]{1,0:T(8,128)S(1)}, f32[8,128,128]{2,1,0:T(8,128)S(1)}) custom-call(f32[8]{0:T(128)} %lam_ref.1, f32[1,128]{1,0:T(1,128)} %bitcast.1, bf16[128,2048]{1,0:T(8,128)(2,1)} %cot_hbm.1, bf16[128,1024]{1,0:T(8,128)(2,1)} %first_hbm.1, ...), custom_call_target="tpu_custom_call" | custom-call | tf_op jit(solution)/shard_map/fused_update/pallas_call | solution.py:541
  120.5 0.8 copy.20
  121.3 0.8 copy.21
  122.1 0.8 copy.23
  122.9 0.8 copy.24
  123.7 2.0 %copy.22 = bf16[2048,1024]{1,0:T(8,128)(2,1)} copy(bf16[2048,1024]{1,0:T(8,128)(2,1)S(1)} %get-tuple-element.7) | data formatting | bytes 8388608

commit v3 on v2

--- a/solution.py
+++ b/solution.py
@@ -301,76 +301,92 @@
     for copy in cot_pair:
         copy.wait_recv()
 
-    lhs = jnp.concatenate([head_in[j] for j in range(inner)], axis=1)
-
-    def part(owner):
+    def head(k):
+        return slice(k * size, (k + 1) * size)
+
+    heads = range(heads_each)
+    lhs = [jnp.concatenate([head_in[j, head(k), :] for j in range(inner)], axis=1) for k in heads]
+
+    def part(owner, k):
         span = pl.ds(pl.multiple_of(owner * chunk, chunk), chunk)
         rhs = cot_all[:, :, span].reshape(inner * rows, chunk)
-        return dot(lhs, rhs, ((1,), (0,)))
-
-    base = expect(4)
-    part_out[0] = part(far).astype(jnp.bfloat16)
-    to_relay = describe(part_out.at[0], part_in.at[3], outer_id(near), base + 3)
-
-    @pl.when(is_mid == 0)
-    def _():
-        to_relay.start()
-
-    part_out[1] = part(across).astype(jnp.bfloat16)
+        return dot(lhs[k], rhs, ((1,), (0,)))
+
     slot = 2 - is_mid
-    send(part_out.at[1], part_in.at[slot], outer_id(across), base + slot)
-    part_out[2] = part(near).astype(jnp.bfloat16)
-    send(part_out.at[2], part_in.at[0], outer_id(near), base)
-    combined = describe(part_out.at[3], part_in.at[1], outer_id(far), base + 1)
-
-    @pl.when(is_mid == 1)
-    def _():
-        arrived(part_in.at[3], base + 3)
-        total_far = part(far) + part_in[3].astype(jnp.float32)
-        part_out[3] = total_far.astype(jnp.bfloat16)
-        combined.start()
-
-    own_part[...] = part(oi)
-    arrived(part_in.at[0], base)
-    own_part[...] += part_in[0].astype(jnp.float32)
-
-    @pl.when(is_mid == 1)
-    def _():
-        arrived(part_in.at[2], base + 2)
-        own_part[...] += part_in[2].astype(jnp.float32)
-
-    arrived(part_in.at[1], base + 1)
-    gradient = own_part[...] + part_in[1].astype(jnp.float32)
-    grad_t[oi] = gradient.astype(jnp.bfloat16)
-    wait_near, wait_far, wait_across = gather_outer(lambda o: grad_t.at[o])
-    square_out[0, 0] = jnp.full((8, 128), jnp.sum(gradient * gradient), jnp.float32)
-    grad_rows[...] = gradient.T.astype(jnp.bfloat16)
+    bases, to_relay, combined = [], [], []
+    for k in heads:
+        base = expect(4)
+        bases.append(base)
+        part_out[k, 0] = part(far, k).astype(jnp.bfloat16)
+        copy = describe(part_out.at[k, 0], part_in.at[k, 3], outer_id(near), base + 3)
+        to_relay.append(copy)
+
+        @pl.when(is_mid == 0)
+        def _():
+            copy.start()
+
+        part_out[k, 1] = part(across, k).astype(jnp.bfloat16)
+        send(part_out.at[k, 1], part_in.at[k, slot], outer_id(across), base + slot)
+        part_out[k, 2] = part(near, k).astype(jnp.bfloat16)
+        send(part_out.at[k, 2], part_in.at[k, 0], outer_id(near), base)
+    for k in heads:
+        copy = describe(part_out.at[k, 3], part_in.at[k, 1], outer_id(far), bases[k] + 1)
+        combined.append(copy)
+
+        @pl.when(is_mid == 1)
+        def _():
+            arrived(part_in.at[k, 3], bases[k] + 3)
+            total_far = part_out[k, 0].astype(jnp.float32) + part_in[k, 3].astype(jnp.float32)
+            part_out[k, 3] = total_far.astype(jnp.bfloat16)
+            copy.start()
+
+    for k in heads:
+        own_part[k] = part(oi, k)
+    grad_square = jnp.zeros((), jnp.float32)
+    grad_waits = []
+    for k in heads:
+        base = bases[k]
+        arrived(part_in.at[k, 0], base)
+        own_part[k] += part_in[k, 0].astype(jnp.float32)
+
+        @pl.when(is_mid == 1)
+        def _():
+            arrived(part_in.at[k, 2], base + 2)
+            own_part[k] += part_in[k, 2].astype(jnp.float32)
+
+        arrived(part_in.at[k, 1], base + 1)
+        gradient = own_part[k] + part_in[k, 1].astype(jnp.float32)
+        own_part[k] = gradient
+        grad_t[oi, head(k), :] = gradient.astype(jnp.bfloat16)
+        grad_waits.append(gather_outer(lambda o, k=k: grad_t.at[o, head(k), :]))
+    for k in heads:
+        gradient = own_part[k]
+        grad_square = grad_square + jnp.sum(gradient * gradient)
+        grad_rows[:, head(k)] = gradient.T.astype(jnp.bfloat16)
+    square_out[0, 0] = jnp.full((8, 128), grad_square, jnp.float32)
 
     root_pair = forward(root_copies, root_all)
-    wait_far()
+    grad_waits[0][1]()
     for copy in root_pair:
         copy.wait_recv()
     locals_[2].wait()
-    wait_near()
-    wait_across()
 
     total = jnp.zeros((1, 1), jnp.float32)
-    pre_copies = []
-    for d in tuple(inner_steps) + (0,):
-        block = inner_peer(d)
-        acc = jnp.zeros((own_rows, cols), jnp.float32)
+    for k in heads:
+        wait_near, wait_far, wait_across = grad_waits[k]
+        wait_near()
+        wait_across()
+        if k + 1 < heads_each:
+            grad_waits[k + 1][1]()
+        acc = jnp.zeros((inner * own_rows, size), jnp.float32)
         for o in range(outer):
-            acc = acc + dot(
-                root_all[block, :, o * chunk : (o + 1) * chunk], grad_t[o], ((1,), (1,))
-            )
-        left_half = acc.astype(jnp.bfloat16)
-        for k in range(heads_each):
-            span = slice(k * size, (k + 1) * size)
-            precond = dot(left_half[:, span], rr_ref[ij * heads_each + k], ((1,), (0,)))
-            total = total + jnp.sum(precond * precond)
-            pre_out[block, :, span] = precond.astype(jnp.bfloat16)
-        if d:
-            pre_copies.append(send(pre_out.at[block], pre_in.at[ij], inner_id(d)))
+            block = root_all[:, :, o * chunk : (o + 1) * chunk].reshape(inner * own_rows, chunk)
+            acc = acc + dot(block, grad_t[o, head(k), :], ((1,), (1,)))
+        precond = dot(acc.astype(jnp.bfloat16), rr_ref[ij * heads_each + k], ((1,), (0,)))
+        total = total + jnp.sum(precond * precond)
+        for j in range(inner):
+            pre_out[j, :, head(k)] = precond[j * own_rows : (j + 1) * own_rows].astype(jnp.bfloat16)
+    pre_copies = [send(pre_out.at[inner_peer(d)], pre_in.at[ij], inner_id(d)) for d in inner_steps]
     pre_in[ij] = pre_out[ij]
     square_out[0, 1] = jnp.broadcast_to(total, (8, 128))
     square_copy = send(square_out.at[0], square_in.at[0], sibling)
@@ -441,43 +457,57 @@
         step_ref[:, span] = step
         new_weight_ref[:, span] = updated
         copy_ref[place, span] = updated.astype(jnp.bfloat16)
-    near_in, far_in, across_in = gather_outer(lambda o: copy_ref.at[rows_of(o, ij), :])
-
-    def halves(o, j):
-        start = (o * inner + j) * own_rows
-        return [
-            copy_ref.at[pl.ds(pl.multiple_of(start + k * (own_rows // 2), own_rows // 2), own_rows // 2), :]
-            for k in range(2)
-        ]
-
-    flight = []
-
-    def spread(o):
-        block = copy_ref.at[rows_of(o, ij), :]
-        flight.append((o, send(block, block, inner_at(x_peer)), send(block, block, inner_at(y_peer))))
+    main = own_rows * 3 // 4
+    rest = own_rows - main
+
+    def piece(o, j, start, count):
+        place = (o * inner + j) * own_rows + start
+        return copy_ref.at[pl.ds(pl.multiple_of(place, own_rows // 8), count), :]
 
     last = []
 
-    def pass_on(index):
-        o, from_x, from_y = flight[index]
+    def spread(o, start, count):
+        block = piece(o, ij, start, count)
+        to_x = send(block, block, inner_at(x_peer))
+        to_y = send(block, block, inner_at(y_peer))
+        return o, start, count, to_x, to_y
+
+    def pass_on(flight):
+        o, start, count, from_x, from_y = flight
+        part_rows = count // 2
         from_x.wait_recv()
-        piece = halves(o, x_peer)[0]
-        last.append(send(piece, piece, inner_at(y_peer)))
+        block = piece(o, x_peer, start, part_rows)
+        one = send(block, block, inner_at(y_peer))
         from_y.wait_recv()
-        piece = halves(o, y_peer)[1]
-        last.append(send(piece, piece, inner_at(x_peer)))
-
-    spread(oi)
+        block = piece(o, y_peer, start + part_rows, part_rows)
+        return one, send(block, block, inner_at(x_peer))
+
+    def gather_rest(j):
+        return gather_outer(lambda o: piece(o, j, main, rest))
+
+    rest_flight = spread(oi, main, rest)
+    near_in, far_in, across_in = gather_outer(lambda o: piece(o, ij, 0, main))
+    flight = spread(oi, 0, main)
+    rest_waits = [gather_rest(ij)]
+    rest_last = pass_on(rest_flight)
+    rest_waits += [gather_rest(x_peer), gather_rest(y_peer)]
     near_in()
-    spread(near)
-    pass_on(0)
+    near_flight = spread(near, 0, main)
     far_in()
+    last += pass_on(flight)
+    for copy in rest_last:
+        copy.wait_recv()
+    rest_waits.append(gather_rest(inner - 1 - ij))
     across_in()
-    spread(across)
-    pass_on(1)
-    spread(far)
-    pass_on(2)
-    pass_on(3)
+    across_flight = spread(across, 0, main)
+    rest_waits[0][1]()
+    far_flight = spread(far, 0, main)
+    last += pass_on(near_flight)
+    rest_waits[1][1]()
+    rest_waits[2][1]()
+    last += pass_on(across_flight)
+    rest_waits[3][1]()
+    last += pass_on(far_flight)
 
     for copy in prod_copies:
         copy.wait_recv()
@@ -498,18 +528,21 @@
     new_left_ref[...] = decay_rate * ls_ref[...] + scale * stat_sum
     for copy in last:
         copy.wait_recv()
+    for near_in, _, across_in in rest_waits:
+        near_in()
+        across_in()
     for copy in started:
         copy.wait_send()
 
     @pl.when(is_mid == 1)
     def _():
-        combined.wait_send()
-        for copy in started_mid:
+        for copy in combined + started_mid:
             copy.wait_send()
 
     @pl.when(is_mid == 0)
     def _():
-        to_relay.wait_send()
+        for copy in to_relay:
+            copy.wait_send()
 
 
 def fused(
@@ -537,7 +570,7 @@
     bf16, f32 = jnp.bfloat16, jnp.float32
     vmem = pl.BlockSpec(memory_space=pltpu.VMEM)
     anywhere = pl.BlockSpec(memory_space=pl.ANY)
-    copies = 12 * inner + 5 * outer + 4 * outer
+    copies = (20 + 6 * heads_each) * inner
     return pl.pallas_call(
         functools.partial(fused_kernel, outer, inner),
         out_shape=(
@@ -554,9 +587,9 @@
             pltpu.VMEM((inner, own_rows, width), bf16),
             pltpu.VMEM((inner, cols, rows), bf16),
             pltpu.VMEM((inner, cols, rows), bf16),
-            pltpu.VMEM((outer, cols, chunk), bf16),
-            pltpu.VMEM((outer, cols, chunk), bf16),
-            pltpu.VMEM((cols, chunk), f32),
+            pltpu.VMEM((heads_each, outer, size, chunk), bf16),
+            pltpu.VMEM((heads_each, outer, size, chunk), bf16),
+            pltpu.VMEM((heads_each, size, chunk), f32),
             pltpu.VMEM((outer, cols, chunk), bf16),
             pltpu.VMEM((chunk, cols), bf16),
             pltpu.VMEM((inner, own_rows, cols), bf16),
@@ -607,7 +640,7 @@
         and head_count % INNER == 0
         and size == 128
         and args[0].shape[0] % 128 == 0
-        and args[5].shape[0] % 16 == 0
+        and args[5].shape[0] % 128 == 0
         and (args[0].shape[1] // outer) % 128 == 0
     )
     return tuple(fused(*args)) if aligned else shards(*args)

time: 126 us -> 118 us (0.937)
  Pallas kernels: 120 us -> 112 us
    pallas_call x1, Pallas kernels: 120 us -> 112 us  [fused(): pl.pallas_call(functools.partial(fused_kernel, outer, inner), out_shape=(...]
where the time goes in v3:
time: 118 us
  Pallas kernels  112 us (95%)
  local copies, waits for them, and re-layouts  5.19 us (4%)
    pallas_call x1, Pallas kernels, fused(): pl.pallas_call(functools.partial(fused_kernel, outer, inner), out_shape=(...  112 us
    unnamed x5, local copies, waits for them, and re-layouts  5.19 us

profile of v3, /device:TPU:0, one launch (start us, length us, event | category | flops | bytes accessed | tf_op | source)
XLA Modules:
  0.0 117.8 jit_solution(7019451650905519856)
XLA Ops:
  0.6 112.0 %fused_update.1 = (f32[128,1024]{1,0:T(8,128)S(1)}, f32[128,1024]{1,0:T(8,128)S(1)}, bf16[2048,1024]{1,0:T(8,128)(2,1)S(1)}, f32[128,1024]{1,0:T(8,128)S(1)}, f32[8,128,128]{2,1,0:T(8,128)S(1)}) custom-call(f32[8]{0:T(128)} %lam_ref.1, f32[1,128]{1,0:T(1,128)} %bitcast.1, bf16[128,2048]{1,0:T(8,128)(2,1)} %cot_hbm.1, bf16[128,1024]{1,0:T(8,128)(2,1)} %first_hbm.1, ...), custom_call_target="tpu_custom_call" | custom-call | tf_op jit(solution)/shard_map/fused_update/pallas_call | solution.py:574
  112.6 0.8 copy.20
  113.4 0.8 copy.21
  114.2 0.8 copy.23
  115.0 0.8 copy.24
  115.8 2.0 %copy.22 = bf16[2048,1024]{1,0:T(8,128)(2,1)} copy(bf16[2048,1024]{1,0:T(8,128)(2,1)S(1)} %get-tuple-element.7) | data formatting | bytes 8388608

commit v4 on v3

--- a/solution.py
+++ b/solution.py
@@ -457,7 +457,7 @@
         step_ref[:, span] = step
         new_weight_ref[:, span] = updated
         copy_ref[place, span] = updated.astype(jnp.bfloat16)
-    main = own_rows * 3 // 4
+    main = own_rows * 5 // 8
     rest = own_rows - main
 
     def piece(o, j, start, count):
@@ -472,14 +472,17 @@
         to_y = send(block, block, inner_at(y_peer))
         return o, start, count, to_x, to_y
 
-    def pass_on(flight):
+    def pass_on(flight, flip=False):
         o, start, count, from_x, from_y = flight
-        part_rows = count // 2
+        unit = own_rows // 8
+        part_rows = (count // unit + 1) // 2 * unit
+        if flip:
+            part_rows = count - part_rows
         from_x.wait_recv()
         block = piece(o, x_peer, start, part_rows)
         one = send(block, block, inner_at(y_peer))
         from_y.wait_recv()
-        block = piece(o, y_peer, start + part_rows, part_rows)
+        block = piece(o, y_peer, start + part_rows, count - part_rows)
         return one, send(block, block, inner_at(x_peer))
 
     def gather_rest(j):
@@ -494,7 +497,7 @@
     near_in()
     near_flight = spread(near, 0, main)
     far_in()
-    last += pass_on(flight)
+    last += pass_on(flight, True)
     for copy in rest_last:
         copy.wait_recv()
     rest_waits.append(gather_rest(inner - 1 - ij))
@@ -505,7 +508,7 @@
     last += pass_on(near_flight)
     rest_waits[1][1]()
     rest_waits[2][1]()
-    last += pass_on(across_flight)
+    last += pass_on(across_flight, True)
     rest_waits[3][1]()
     last += pass_on(far_flight)
 

time: 118 us -> 121 us (1.025)
  Pallas kernels: 112 us -> 115 us
    pallas_call x1, Pallas kernels: 112 us -> 115 us  [fused(): pl.pallas_call(functools.partial(fused_kernel, outer, inner), out_shape=(...]
where the time goes in v4:
time: 121 us
  Pallas kernels  115 us (95%)
  local copies, waits for them, and re-layouts  5.19 us (4%)
    pallas_call x1, Pallas kernels, fused(): pl.pallas_call(functools.partial(fused_kernel, outer, inner), out_shape=(...  115 us
    unnamed x5, local copies, waits for them, and re-layouts  5.19 us

profile of v4, /device:TPU:0, one launch (start us, length us, event | category | flops | bytes accessed | tf_op | source)
XLA Modules:
  0.0 120.7 jit_solution(12423881889117850544)
XLA Ops:
  0.6 114.8 %fused_update.1 = (f32[128,1024]{1,0:T(8,128)S(1)}, f32[128,1024]{1,0:T(8,128)S(1)}, bf16[2048,1024]{1,0:T(8,128)(2,1)S(1)}, f32[128,1024]{1,0:T(8,128)S(1)}, f32[8,128,128]{2,1,0:T(8,128)S(1)}) custom-call(f32[8]{0:T(128)} %lam_ref.1, f32[1,128]{1,0:T(1,128)} %bitcast.1, bf16[128,2048]{1,0:T(8,128)(2,1)} %cot_hbm.1, bf16[128,1024]{1,0:T(8,128)(2,1)} %first_hbm.1, ...), custom_call_target="tpu_custom_call" | custom-call | tf_op jit(solution)/shard_map/fused_update/pallas_call | solution.py:577
  115.5 0.8 copy.20
  116.3 0.8 copy.21
  117.1 0.8 copy.23
  117.9 0.8 copy.24
  118.7 2.0 %copy.22 = bf16[2048,1024]{1,0:T(8,128)(2,1)} copy(bf16[2048,1024]{1,0:T(8,128)(2,1)S(1)} %get-tuple-element.7) | data formatting | bytes 8388608
